TPU v7x, 128 devices: a whole 4x4x4 slice. The times are simulated.
128 devices in a mesh: sp: 16 (over z, y), tp: 8 (over x, core).
Axes of the slice: x: 4, y: 4, z: 4, core: 2. Of those that a mesh axis runs over, the one named last changes fastest.
Arguments:
- skip_stream_vector: bfloat16 [16384, 2048], P(('sp', 'tp')), may hold values from -6 to 6
- probe_preactivation: bfloat16 [16384, 1024], P('sp', 'tp'), may hold values from -6 to 6
- retention_preactivation: bfloat16 [16384, 1024], P('sp', 'tp'), may hold values from -4.5 to 4.5
- content_vector: bfloat16 [16384, 1024], P('sp', 'tp'), may hold values from -6 to 6
- emission_preactivation: bfloat16 [16384, 1024], P('sp', 'tp'), may hold values from -6 to 6
- retention_slack: float32 [1024], P('tp'), may hold values from 0 to 0.12
- surge_rate: float32 [16384, 1024], P('sp', 'tp'), may hold values from -1.2 to 0
- subspace_scaling_factor: float32 [1024], P('tp'), may hold values from 0.1 to 1.9
- emission_matrix: bfloat16 [1024, 2048], replicated, may hold values from -0.1875 to 0.1875
- mlp_scaling_factor: float32 [2048], replicated, may hold values from 0.1 to 1.9
- switch_matrix: bfloat16 [2048, 5632], P('sp', 'tp'), may hold values from -0.125 to 0.125
- expansion_matrix: bfloat16 [2048, 5632], P('sp', 'tp'), may hold values from -0.125 to 0.125
- contraction_matrix: bfloat16 [5632, 2048], P('tp', 'sp'), may hold values from -0.078125 to 0.078125
Outputs:
- stream_out: bfloat16 [16384, 2048], P(('sp', 'tp'))
All inputs are finite; a program needn't handle non-finite values.
Results may differ from a plain program's by a relative error of at most 0.017.
Values may be sent and summed in bfloat16 or wider, within the bound.
A program may use at most 128 MiB of HBM per device.

v0:
```python
import jax
import jax.numpy as jnp
from jax import lax
from jax.sharding import Mesh
from jax.sharding import PartitionSpec as P

HEAD_DIM = 128
BLOCK = 64
TP = ("tp_0", "tp_1")
SP_TP = ("sp", "tp_0", "tp_1")
EPSILON = 1e-06
TOP_PRECISION = lax.Precision.HIGHEST


def in_one_piece(arrays, axis, dim, along):
    both = jnp.concatenate(arrays, axis=along)
    whole, at, outs = (lax.all_gather(both, axis, axis=dim, tiled=True), 0, [])
    for a in arrays:
        outs.append(lax.slice_in_dim(whole, at, at + a.shape[along], axis=along))
        at += a.shape[along]
    return tuple(outs)


def from_everyone(value, axis):
    peers = lax.axis_size(axis)
    return lax.all_to_all(
        jnp.broadcast_to(value[None], (peers, *value.shape)), axis, 0, 0, tiled=True
    )


def all_in_one(value, axis):
    leaves = jax.tree.leaves(value)
    order = sorted(range(len(leaves)), key=lambda k: -leaves[k].size)
    width = (1, *leaves[order[0]].shape)[-1]
    lines = [
        jnp.pad(leaves[k].reshape(-1), (0, -leaves[k].size % width)).reshape(-1, width)
        for k in order
    ]
    both, at, found = (from_everyone(jnp.concatenate(lines), axis), 0, {})
    for k, line in zip(order, lines):
        piece = both[:, at : at + len(line)].reshape(len(both), -1)
        found[k] = piece[:, : leaves[k].size].reshape(-1, *leaves[k].shape)
        at += len(line)
    numbers = iter(range(len(leaves)))
    return jax.tree.map(lambda _: found[next(numbers)], value)


def joined_by_halves(pieces, combine):
    while len(jax.tree.leaves(pieces)[0]) > 1:
        pieces = jax.vmap(combine)(
            *(jax.tree.map(lambda part: part[side::2], pieces) for side in (0, 1))
        )
    return jax.tree.map(lambda part: part[0], pieces)


def carried_in(value, axis, combine, identity):
    peers, here = (lax.axis_size(axis), lax.axis_index(axis))
    passed = jnp.arange(peers) < here

    def kept(part, zero, own):
        part = jnp.where(
            passed.reshape(-1, *(1 for _ in own.shape)),
            part.astype(own.dtype),
            jnp.asarray(zero, own.dtype),
        )
        return part

    pieces = all_in_one(
        jax.tree.map(lambda part, kind: part.astype(kind), value, (jnp.bfloat16, jnp.bfloat16)),
        axis,
    )
    return joined_by_halves(jax.tree.map(kept, pieces, identity, value), combine)


def joined_along(tiles, dim):
    lengths = list(tiles.shape[1:])
    lengths[dim] *= tiles.shape[0]
    return jnp.moveaxis(tiles, 0, dim).reshape(lengths)


def gathered_by_axis(value, axes, dim):
    far, near = axes
    tiles = from_everyone(from_everyone(value, far), near)
    return joined_along(tiles.swapaxes(0, 1).reshape(-1, *value.shape), dim)


def in_blocks(value, dim, peers):
    lengths = value.shape
    tiles = value.reshape(*lengths[:dim], peers, lengths[dim] // peers, *lengths[dim + 1 :])
    return jnp.moveaxis(tiles, dim, 0)


def summed_on_arrival(value, axis, dim):
    tiles = in_blocks(value, dim, lax.axis_size(axis))
    arrived = lax.all_to_all(tiles, axis, split_axis=0, concat_axis=0, tiled=True)
    return arrived.astype(jnp.float32).sum(axis=0)


def sum_by_axis(value, axes, dim):
    far, near = axes
    own = summed_on_arrival(in_blocks(value, dim, lax.axis_size(far)), near, dim + 1)
    return jnp.sum(
        lax.all_to_all(own.astype(jnp.bfloat16), far, 0, 0, tiled=True).astype(jnp.float32), axis=0
    )


def block_step(carry, inputs):
    memory_state, offsets = carry
    query_block, input_gate_block, value_block, log_blk = inputs
    cumulative_decay = jnp.cumsum(log_blk, axis=1)
    length = log_blk.shape[1]
    carried_share = jnp.einsum(
        "eia,eax->eix",
        query_block * jnp.exp(cumulative_decay),
        memory_state,
        precision=TOP_PRECISION,
    )
    middle = cumulative_decay[:, length // 2, :][:, None, :]
    left_side = query_block * jnp.exp(cumulative_decay - middle)
    right_side = input_gate_block * jnp.exp(middle - cumulative_decay)
    causal = (jnp.arange(length)[:, None] >= jnp.arange(length)[None, :])[None, :, :]
    scores = jnp.einsum("htk,hsk->hts", left_side, right_side, precision=TOP_PRECISION)
    scores = jnp.where(causal, scores, 0.0)
    outputs = carried_share + jnp.einsum(
        "hts,hsv->htv", scores, value_block, precision=TOP_PRECISION
    )
    closing_log_decay = cumulative_decay[:, -1, :]
    updated_memory_state = jnp.exp(closing_log_decay)[:, :, None] * memory_state + jnp.einsum(
        "qnj,qnl->qjl",
        input_gate_block * jnp.exp(closing_log_decay[:, None, :] - cumulative_decay),
        value_block,
        precision=TOP_PRECISION,
    )
    return (
        (updated_memory_state, offsets + closing_log_decay),
        (outputs, cumulative_decay + offsets[:, None, :]),
    )


def split_blocks(values, heads_here):
    count = values.shape[0]
    return values.reshape(count // BLOCK, BLOCK, heads_here, HEAD_DIM).transpose(0, 2, 1, 3)


def admission_source_matrix(
    probe_preactivation, retention_preactivation, content_vector, retention_slack, surge_rate
):
    query_act = jax.nn.silu(probe_preactivation.astype(jnp.float32))
    admission_factor = retention_slack[None, :] * jax.nn.sigmoid(
        -retention_preactivation.astype(jnp.float32)
    )
    retention_logarithm = jnp.log1p(-admission_factor) + surge_rate
    return (query_act, admission_factor, content_vector.astype(jnp.float32), retention_logarithm)


def head_output(outputs, subspace_scaling_factor, emission_preactivation):
    count, heads_here = (outputs.shape[0], outputs.shape[1])
    squares = jnp.mean(outputs * outputs, axis=-1, keepdims=True)
    scaled = (
        outputs
        * lax.rsqrt(squares + EPSILON)
        * subspace_scaling_factor.reshape(heads_here, HEAD_DIM)
    )
    scaled = scaled.reshape(count, heads_here * HEAD_DIM)
    return (scaled * jax.nn.silu(emission_preactivation.astype(jnp.float32))).astype(jnp.bfloat16)


def row_norm(stream, mlp_scaling_factor):
    streamf = stream.astype(jnp.float32)
    squares = jnp.mean(streamf * streamf, axis=-1, keepdims=True)
    return (streamf * lax.rsqrt(squares + EPSILON) * mlp_scaling_factor).astype(jnp.bfloat16)


def chain(earlier, later):
    return (earlier[0] * later[0], later[0][:, :, None] * earlier[1] + later[1])


def on_device(
    skip_stream_vector,
    probe_preactivation,
    retention_preactivation,
    content_vector,
    emission_preactivation,
    retention_slack,
    surge_rate,
    subspace_scaling_factor,
    emission_matrix,
    mlp_scaling_factor,
    switch_matrix,
    expansion_matrix,
    contraction_matrix,
):
    gate_whole, up_whole = in_one_piece((switch_matrix, expansion_matrix), "sp", 0, 1)
    down_whole = lax.all_gather(contraction_matrix, "sp", axis=1, tiled=True)
    heads_here = probe_preactivation.shape[1] // HEAD_DIM
    tok_rows = probe_preactivation.shape[0]
    arranged_sources = admission_source_matrix(
        probe_preactivation, retention_preactivation, content_vector, retention_slack, surge_rate
    )
    block_list = tuple((split_blocks(item, heads_here) for item in arranged_sources))
    start_carry = (
        jnp.zeros((heads_here, HEAD_DIM, HEAD_DIM), jnp.float32),
        jnp.zeros((heads_here, HEAD_DIM), jnp.float32),
    )
    (memory_state, offsets), (outputs, cumulative_log_decay) = lax.scan(
        block_step, start_carry, block_list
    )
    incoming_state = carried_in(
        (jnp.exp(offsets), memory_state),
        "sp",
        chain,
        (jnp.ones_like(offsets), jnp.zeros_like(memory_state)),
    )
    outputs = outputs + jnp.einsum(
        "jmxo,mos->jmxs",
        block_list[0] * jnp.exp(cumulative_log_decay),
        incoming_state[1],
        precision=TOP_PRECISION,
    )
    outputs = outputs.transpose(0, 2, 1, 3).reshape(tok_rows, heads_here, HEAD_DIM)
    mixed = head_output(outputs, subspace_scaling_factor, emission_preactivation)
    regrouped = lax.all_to_all(mixed, TP, split_axis=0, concat_axis=1, tiled=True)
    projected = jnp.dot(regrouped, emission_matrix, preferred_element_type=jnp.float32)
    stream = (skip_stream_vector.astype(jnp.float32) + projected).astype(jnp.bfloat16)
    normed = row_norm(stream, mlp_scaling_factor)
    all_rows = gathered_by_axis(normed, ("tp_0", "tp_1"), 0)
    gate_proj = jnp.dot(all_rows, gate_whole, preferred_element_type=jnp.float32)
    up_proj = jnp.dot(all_rows, up_whole, preferred_element_type=jnp.float32)
    hidden = (jax.nn.silu(gate_proj) * up_proj).astype(jnp.bfloat16)
    partial_sum = jnp.dot(hidden, down_whole, preferred_element_type=jnp.float32)
    summed = sum_by_axis(partial_sum.astype(jnp.bfloat16), ("tp_0", "tp_1"), 0)
    return (stream.astype(jnp.float32) + summed).astype(jnp.bfloat16)


def solution(mesh):
    split = Mesh(mesh.devices.reshape(mesh.shape["sp"], 4, 2), ("sp", "tp_0", "tp_1"))
    return jax.shard_map(
        on_device,
        mesh=split,
        in_specs=(
            P(SP_TP, None),
            P("sp", TP),
            P("sp", TP),
            P("sp", TP),
            P("sp", TP),
            P(TP),
            P("sp", TP),
            P(TP),
            P(),
            P(),
            P("sp", TP),
            P("sp", TP),
            P(TP, "sp"),
        ),
        out_specs=P(SP_TP, None),
        check_vma=False,
    )
```

profile of v0, /device:TPU:0, one launch (start us, length us, event | category | flops | bytes accessed | tf_op | source)
XLA Modules:
  0.0 193.7 jit_solution(10395686392634396452)
XLA Ops:
  6.5 1.8 pad_maximum_fusion
  8.4 1.1 convert_multiply_fusion.1
  9.5 1.0 convert.2
  10.5 1.5 divide_multiply_fusion
  12.0 17.0 %while.17 = (s32[]{:T(128)}, f32[1,128,128]{2,1,0:T(8,128)S(1)}, f32[1,128]{1,0:T(1,128)S(1)}, f32[16,1,64,128]{3,2,1,0:T(8,128)S(1)}, f32[16,1,64,128]{3,2,1,0:...) while((s32[]{:T(128)}, f32[1,128,128]{2,1,0:T(8,128)S(1)}, ...), condition=%wide.region_2.3_spmd.clone, body=%wide.region_0.2_spmd.clone.sunk | while | flops 38412544 | bytes 879768 | solution.py:205
  12.1 0.2 convolution_select_fusion.2
  12.5 0.3 fusion.99
  13.2 0.2 convolution_select_fusion.2
  13.4 0.2 fusion.101
  13.6 0.3 fusion.99
  14.3 0.2 convolution_select_fusion.2
  14.5 0.2 fusion.101
  14.7 0.3 fusion.99
  15.3 0.2 convolution_select_fusion.2
  15.5 0.2 fusion.101
  15.7 0.3 fusion.99
  16.4 0.2 convolution_select_fusion.2
  16.8 0.3 fusion.99
  17.4 0.2 convolution_select_fusion.2
  17.7 0.2 fusion.101
  17.8 0.3 fusion.99
  18.5 0.2 convolution_select_fusion.2
  18.9 0.3 fusion.99
  19.6 0.2 convolution_select_fusion.2
  20.0 0.3 fusion.99
  20.6 0.2 convolution_select_fusion.2
  21.0 0.3 fusion.99
  21.7 0.2 convolution_select_fusion.2
  22.1 0.3 fusion.99
  22.8 0.2 convolution_select_fusion.2
  23.2 0.3 fusion.99
  23.8 0.2 convolution_select_fusion.2
  24.2 0.3 fusion.99
  24.9 0.2 convolution_select_fusion.2
  25.3 0.3 fusion.99
  25.9 0.2 convolution_select_fusion.2
  26.3 0.3 fusion.99
  27.0 0.2 convolution_select_fusion.2
  27.4 0.3 fusion.99
  28.1 0.2 convolution_select_fusion.2
  28.5 0.3 fusion.99
  29.0 0.9 broadcast_in_dim.48
  29.9 8.2 %all-to-all-start = ((bf16[16,129,128]{2,1,0:T(8,128)(2,1)}), bf16[16,129,128]{2,1,0:T(8,128)(2,1)S(1)}, u32[]{:S(2)}, u32[]{:S(2)}) async-start(bf16[16,129,128]{2,1,0:T(8,128)(2,1)} %broadcast_in_dim.48), calls=%async_computation | async-start | bytes 1114112 | tf_op jit(solution)/shard_map/all_to_all | solution.py:26
  38.1 0.7 all-gather.5.cloned.1.call-update
  38.9 11.2 %all-to-all-done = bf16[16,129,128]{2,1,0:T(8,128)(2,1)S(1)} async-done(((bf16[16,129,128]{2,1,0:T(8,128)(2,1)}), bf16[16,129,128]{2,1,0:T(8,128)(2,1)S(1)}, u32[]{:S(2)}, u32[]{:S(2)}) %all-to-all-start) | async-done | bytes 528416 | tf_op jit(solution)/shard_map/all_to_all | solution.py:26
  50.4 0.2 slice_add_fusion
  50.8 0.7 multiply_reduce_fusion.1
  51.7 0.2 fusion.63
  51.9 11.6 %all_to_all.44 = bf16[8,128,128]{2,1,0:T(8,128)(2,1)S(1)} all-to-all(bf16[8,128,128]{2,1,0:T(8,128)(2,1)S(1)} %bitcast.185), channel_id=1, replica_groups=mesh['sp'=16,'tp_0'=4,'tp_1'=2] {'tp_0','tp_1'}, dimensions={0} | all-to-all | bytes 524288 | tf_op jit(solution)/shard_map/all_to_all | solution.py:222
  63.7 3.0 %multiply_reduce_fusion = (f32[128]{0:T(128)S(1)}, f32[128,2048]{1,0:T(8,128)S(1)}) fusion(bf16[128,1024]{0,1:T(8,128)(2,1)S(1)} %bitcast.183, bf16[1024,2048]{1,0:T(8,128)(2,1)} %param.23, bf16[128,2048]{1,0:T(8,128)(2,1)S(1)} %copy-done), kind=kOutput, calls=%fused_computation.66 | convolution fusion | flops 538443648 | bytes 6029824 | tf_op jit(solution)/shard_map/dot_general | solution.py:223
  66.9 0.2 broadcast_in_dim.74
  67.1 28.8 %all_to_all.45 = bf16[4,128,2048]{2,1,0:T(8,128)(2,1)S(1)} all-to-all(bf16[4,128,2048]{2,1,0:T(8,128)(2,1)S(1)} %broadcast_in_dim.74), channel_id=1, replica_groups=mesh['sp'=16,'tp_0'=4,'tp_1'=2] {'tp_0'}, dimensions={0} | all-to-all | bytes 4194304 | tf_op jit(solution)/shard_map/all_to_all | solution.py:26
  95.9 0.5 broadcast_in_dim.75
  96.5 7.1 %all_to_all.46 = bf16[2,4,128,2048]{3,2,1,0:T(8,128)(2,1)S(1)} all-to-all(bf16[2,4,128,2048]{3,2,1,0:T(8,128)(2,1)S(1)} %broadcast_in_dim.75), channel_id=1, replica_groups=mesh['sp'=16,'tp_0'=4,'tp_1'=2] {'tp_1'}, dimensions={0} | all-to-all | bytes 8388608 | tf_op jit(solution)/shard_map/all_to_all | solution.py:26
  103.6 2.3 %copy.36 = bf16[2,4,128,2048]{3,2,0,1:T(8,128)(2,1)} copy(bf16[2,4,128,2048]{3,2,1,0:T(8,128)(2,1)S(1)} %all_to_all.46) | data formatting | bytes 8388608 | tf_op jit(solution)/shard_map/all_to_all | solution.py:26
  105.9 7.9 %fusion.43 = f32[1024,704]{0,1:T(8,128)} fusion(bf16[1024,2048]{1,0:T(8,128)(2,1)} %bitcast.178, bf16[2048,1408]{0,1:T(8,128)(2,1)} %all-gather.3.cloned.1.call-done), kind=kOutput, calls=%fused_computation.56 | convolution fusion | flops 2952790016 | bytes 9961472 | tf_op jit(solution)/shard_map/dot_general | solution.py:227
  113.8 14.8 %all-gather.5.cloned.1.call-done = bf16[704,2048]{1,0:T(8,128)(2,1)} async-done(((bf16[704,128]{1,0:T(8,128)(2,1)}), bf16[704,2048]{1,0:T(8,128)(2,1)}) %all-gather.5.cloned.1.call-update) | async-done | bytes 2883600 | tf_op jit(solution)/shard_map/all_gather | solution.py:194
  128.6 12.1 %convolution_convert_fusion = bf16[1024,2048]{1,0:T(8,128)(2,1)} fusion(bf16[704,2048]{1,0:T(8,128)(2,1)} %all-gather.5.cloned.1.call-done, f32[1024,704]{0,1:T(8,128)} %fusion.43, bf16[1024,2048]{1,0:T(8,128)(2,1)} %bitcast.179, bf16[2048,1408]{0,1:T(8,128)(2,1)} %all-gather.3.cloned.1.call-done), kind=kOutput, calls=%fused_computation.53 | convolution fusion | flops 5912002560 | bytes 17039360 | tf_op jit(solution)/shard_map/dot_general | solution.py:230
  140.7 2.5 %copy.39 = bf16[4,2,128,2048]{3,2,0,1:T(8,128)(2,1)S(1)} copy(bf16[4,2,128,2048]{3,2,1,0:T(8,128)(2,1)} %bitcast.180) | data formatting | bytes 8388608 | tf_op jit(solution)/shard_map/reshape;reshape | solution.py:89
  143.2 8.2 %all_to_all.47 = bf16[2,4,128,2048]{3,2,1,0:T(8,128)(2,1)} all-to-all(bf16[2,4,128,2048]{3,2,1,0:T(8,128)(2,1)S(1)} %bitcast.177), channel_id=1, replica_groups=mesh['sp'=16,'tp_0'=4,'tp_1'=2] {'tp_1'}, dimensions={0} | all-to-all | bytes 8388608 | tf_op jit(solution)/shard_map/all_to_all | solution.py:95
  151.3 3.5 %reduce_sum.41 = bf16[4,128,2048]{2,1,0:T(8,128)(2,1)S(1)} reduce(bf16[2,4,128,2048]{3,2,1,0:T(8,128)(2,1)} %all_to_all.47, bf16[]{:T(256)} %constant.49.clone.1), dimensions={0}, to_apply=%region_5.6 | reduce | flops 1048576 | bytes 6291458 | tf_op jit(solution)/shard_map/reduce_sum | solution.py:96
  154.9 30.7 %all_to_all.48 = bf16[4,128,2048]{2,1,0:T(8,128)(2,1)S(1)} all-to-all(bf16[4,128,2048]{2,1,0:T(8,128)(2,1)S(1)} %reduce_sum.41), channel_id=1, replica_groups=mesh['sp'=16,'tp_0'=4,'tp_1'=2] {'tp_0'}, dimensions={0} | all-to-all | bytes 4194304 | tf_op jit(solution)/shard_map/all_to_all | solution.py:103
  185.6 0.4 convert_reduce_fusion
  186.0 0.9 add_convert_fusion
  (157 shorter events, 8.2 us)
Async XLA Ops:
  6.5 99.4 %all-gather.3.cloned.1.call-start = ((), (), s32[]{:S(2)}) async-start(), calls=%async_computation.6 | async-start | bytes 6127616 | tf_op jit(solution)/shard_map/all_gather | solution.py:17
  29.9 20.2 %all-to-all-start = ((bf16[16,129,128]{2,1,0:T(8,128)(2,1)}), bf16[16,129,128]{2,1,0:T(8,128)(2,1)S(1)}, u32[]{:S(2)}, u32[]{:S(2)}) async-start(bf16[16,129,128]{2,1,0:T(8,128)(2,1)} %broadcast_in_dim.48), calls=%async_computation | async-start | bytes 1114112 | tf_op jit(solution)/shard_map/all_to_all | solution.py:26
  38.1 90.5 %all-gather.5.cloned.1.call-start = ((), (), s32[]{:S(2)}) async-start(), calls=%async_computation.7 | async-start | bytes 3063808 | tf_op jit(solution)/shard_map/all_gather | solution.py:194
  50.3 1.3 copy-start.1
  50.3 1.3 copy-start.3
  50.6 13.1 %copy-start = (bf16[128,2048]{1,0:T(8,128)(2,1)S(1)}, bf16[128,2048]{1,0:T(8,128)(2,1)}, u32[]{:S(2)}) copy-start(bf16[128,2048]{1,0:T(8,128)(2,1)} %param.15) | copy-start | bytes 1572868
  63.7 3.0 %copy-start.2 = (f32[2048]{0:T(1024)S(1)}, f32[2048]{0:T(1024)}, u32[]{:S(2)}) copy-start(f32[2048]{0:T(1024)} %param.24) | copy-start | bytes 24580
Sparse Core Ops, SparseCore 0:
  9.4 66.9 all-gather.2
  78.6 49.9 all-gather.4
where the time goes:
time: 194 us
  blocking collectives  86.3 us (44%)
  matrix products  37.4 us (19%)
  waiting for transfers between devices  26.8 us (14%)
  between operations  13.7 us (7%)
  other arithmetic  13.2 us (7%)
  starting transfers between devices  8.21 us (4%)
  local copies, waits for them, and re-layouts  7.13 us (4%)
    all_to_all x2, blocking collectives, from_everyone(): lax.all_to_all(jnp.broadcast_to(value[None], (peers, *value.shape)), axis...  35.9 us
    all_to_all x1, blocking collectives, sum_by_axis(): lax.all_to_all(own.astype(jnp.bfloat16), far, 0, 0, tiled=True)  30.7 us
    all_gather x1, waiting for transfers between devices, on_device(): down_whole = lax.all_gather(contraction_matrix, 'sp', axis=1, tiled=True)  14.8 us
    dot_general x1, matrix products, on_device(): jnp.dot(hidden, down_whole, preferred_element_type=jnp.float32)  12.1 us
    all_to_all x1, blocking collectives, on_device(): lax.all_to_all(mixed, TP, split_axis=0, concat_axis=1, tiled=True)  11.6 us
    all_to_all x1, waiting for transfers between devices, from_everyone(): lax.all_to_all(jnp.broadcast_to(value[None], (peers, *value.shape)), axis...  11.2 us
    all_to_all x1, blocking collectives, summed_on_arrival(): lax.all_to_all(tiles, axis, split_axis=0, concat_axis=0, tiled=True)  8.18 us
    all_to_all x1, starting transfers between devices, from_everyone(): lax.all_to_all(jnp.broadcast_to(value[None], (peers, *value.shape)), axis...  8.16 us
  transfers between devices with their start and end apart: 3, of which 2 were waited for; matrix products, arithmetic and copies ran while one was open for 19% of the time, Pallas kernels for 0%

commit v1 on v0

--- a/solution.py
+++ b/solution.py
@@ -191,7 +191,9 @@
     contraction_matrix,
 ):
     gate_whole, up_whole = in_one_piece((switch_matrix, expansion_matrix), "sp", 0, 1)
-    down_whole = lax.all_gather(contraction_matrix, "sp", axis=1, tiled=True)
+    down_whole = jnp.concatenate(
+        lax.all_to_all(jnp.stack([contraction_matrix] * lax.axis_size("sp")), "sp", 0, 0), axis=1
+    )
     heads_here = probe_preactivation.shape[1] // HEAD_DIM
     tok_rows = probe_preactivation.shape[0]
     arranged_sources = admission_source_matrix(

time: 194 us -> 221 us (1.14)
  waiting for transfers between devices: 26.8 us -> 44.4 us
  local copies, waits for them, and re-layouts: 7.13 us -> 11.8 us
  starting transfers between devices: 8.21 us -> 12.8 us
    all_to_all x0 -> x1, waiting for transfers between devices: none -> 32.4 us  [on_device(): lax.all_to_all(jnp.stack([contraction_matrix] * lax.axis_size('sp')), 'sp...]
    all_gather x1 -> x0, waiting for transfers between devices: 14.8 us -> none  [on_device(): down_whole = lax.all_gather(contraction_matrix, 'sp', axis=1, tiled=True)]
    all_to_all x0 -> x1, starting transfers between devices: none -> 4.64 us  [on_device(): lax.all_to_all(jnp.stack([contraction_matrix] * lax.axis_size('sp')), 'sp...]
    all_to_all x1, local copies, waits for them, and re-layouts: 2.33 us -> 4.8 us  [from_everyone(): lax.all_to_all(jnp.broadcast_to(value[None], (peers, *value.shape)), axis...]
where the time goes in v1:
time: 221 us; the launch traced here: 220 us
  blocking collectives  86.2 us (39%)
  waiting for transfers between devices  44.4 us (20%)
  matrix products  37.4 us (17%)
  between operations  13.7 us (6%)
  other arithmetic  13.1 us (6%)
  starting transfers between devices  12.8 us (6%)
  local copies, waits for them, and re-layouts  11.8 us (5%)
    all_to_all x2, blocking collectives, from_everyone(): lax.all_to_all(jnp.broadcast_to(value[None], (peers, *value.shape)), axis...  37 us
    all_to_all x1, waiting for transfers between devices, on_device(): lax.all_to_all(jnp.stack([contraction_matrix] * lax.axis_size('sp')), 'sp...  32.4 us
    all_to_all x1, blocking collectives, sum_by_axis(): lax.all_to_all(own.astype(jnp.bfloat16), far, 0, 0, tiled=True)  29.4 us
    dot_general x1, matrix products, on_device(): jnp.dot(hidden, down_whole, preferred_element_type=jnp.float32)  12 us
    all_to_all x1, waiting for transfers between devices, from_everyone(): lax.all_to_all(jnp.broadcast_to(value[None], (peers, *value.shape)), axis...  12 us
    all_to_all x1, blocking collectives, on_device(): lax.all_to_all(mixed, TP, split_axis=0, concat_axis=1, tiled=True)  11.6 us
    all_to_all x1, blocking collectives, summed_on_arrival(): lax.all_to_all(tiles, axis, split_axis=0, concat_axis=0, tiled=True)  8.18 us
    all_to_all x1, starting transfers between devices, from_everyone(): lax.all_to_all(jnp.broadcast_to(value[None], (peers, *value.shape)), axis...  8.16 us
  transfers between devices with their start and end apart: 3, of which 2 were waited for; matrix products, arithmetic and copies ran while one was open for 19% of the time, Pallas kernels for 0%

profile of v1, /device:TPU:0, one launch (start us, length us, event | category | flops | bytes accessed | tf_op | source)
XLA Modules:
  0.0 220.4 jit_solution(11975222686143445894)
XLA Ops:
  6.5 1.8 pad_maximum_fusion
  8.4 1.1 convert_multiply_fusion.1
  9.5 1.0 convert.2
  10.5 1.4 divide_multiply_fusion
  11.9 17.0 %while.17 = (s32[]{:T(128)}, f32[1,128,128]{2,1,0:T(8,128)S(1)}, f32[1,128]{1,0:T(1,128)S(1)}, f32[16,1,64,128]{3,2,1,0:T(8,128)S(1)}, f32[16,1,64,128]{3,2,1,0:...) while((s32[]{:T(128)}, f32[1,128,128]{2,1,0:T(8,128)S(1)}, ...), condition=%wide.region_2.3_spmd.clone, body=%wide.region_0.2_spmd.clone.sunk | while | flops 38412544 | bytes 879768 | solution.py:207
  12.1 0.2 convolution_select_fusion.2
  12.5 0.3 fusion.101
  13.1 0.2 convolution_select_fusion.2
  13.3 0.2 fusion.103
  13.5 0.3 fusion.101
  14.2 0.2 convolution_select_fusion.2
  14.4 0.2 fusion.103
  14.6 0.3 fusion.101
  15.3 0.2 convolution_select_fusion.2
  15.7 0.3 fusion.101
  16.3 0.2 convolution_select_fusion.2
  16.7 0.3 fusion.101
  17.4 0.2 convolution_select_fusion.2
  17.6 0.2 fusion.103
  17.8 0.3 fusion.101
  18.5 0.2 convolution_select_fusion.2
  18.9 0.3 fusion.101
  19.5 0.2 convolution_select_fusion.2
  19.9 0.3 fusion.101
  20.6 0.2 convolution_select_fusion.2
  21.0 0.3 fusion.101
  21.6 0.2 convolution_select_fusion.2
  22.0 0.3 fusion.101
  22.7 0.2 convolution_select_fusion.2
  23.1 0.3 fusion.101
  23.8 0.2 convolution_select_fusion.2
  24.2 0.3 fusion.101
  24.8 0.2 convolution_select_fusion.2
  25.2 0.3 fusion.101
  25.9 0.2 convolution_select_fusion.2
  26.3 0.3 fusion.101
  27.0 0.2 convolution_select_fusion.2
  27.4 0.3 fusion.101
  28.0 0.2 convolution_select_fusion.2
  28.4 0.3 fusion.101
  29.0 0.9 broadcast_in_dim.48
  29.9 8.2 %all-to-all-start = ((bf16[16,129,128]{2,1,0:T(8,128)(2,1)}), bf16[16,129,128]{2,1,0:T(8,128)(2,1)S(1)}, u32[]{:S(2)}, u32[]{:S(2)}) async-start(bf16[16,129,128]{2,1,0:T(8,128)(2,1)} %broadcast_in_dim.48), calls=%async_computation | async-start | bytes 1114112 | tf_op jit(solution)/shard_map/all_to_all | solution.py:26
  38.0 12.0 %all-to-all-done = bf16[16,129,128]{2,1,0:T(8,128)(2,1)S(1)} async-done(((bf16[16,129,128]{2,1,0:T(8,128)(2,1)}), bf16[16,129,128]{2,1,0:T(8,128)(2,1)S(1)}, u32[]{:S(2)}, u32[]{:S(2)}) %all-to-all-start) | async-done | bytes 528416 | tf_op jit(solution)/shard_map/all_to_all | solution.py:26
  50.3 0.2 slice_add_fusion
  50.8 0.7 multiply_reduce_fusion.1
  51.6 0.2 fusion.65
  51.8 11.6 %all_to_all.49 = bf16[8,128,128]{2,1,0:T(8,128)(2,1)S(1)} all-to-all(bf16[8,128,128]{2,1,0:T(8,128)(2,1)S(1)} %bitcast.192), channel_id=1, replica_groups=mesh['sp'=16,'tp_0'=4,'tp_1'=2] {'tp_0','tp_1'}, dimensions={0} | all-to-all | bytes 524288 | tf_op jit(solution)/shard_map/all_to_all | solution.py:224
  63.6 3.0 %multiply_reduce_fusion = (f32[128]{0:T(128)S(1)}, f32[128,2048]{1,0:T(8,128)S(1)}) fusion(bf16[128,1024]{0,1:T(8,128)(2,1)S(1)} %bitcast.190, bf16[1024,2048]{1,0:T(8,128)(2,1)} %param.23, bf16[128,2048]{1,0:T(8,128)(2,1)S(1)} %copy-done), kind=kOutput, calls=%fused_computation.68 | convolution fusion | flops 538443648 | bytes 6029824 | tf_op jit(solution)/shard_map/dot_general | solution.py:225
  66.8 0.2 broadcast_in_dim.74
  67.1 28.8 %all_to_all.50 = bf16[4,128,2048]{2,1,0:T(8,128)(2,1)S(1)} all-to-all(bf16[4,128,2048]{2,1,0:T(8,128)(2,1)S(1)} %broadcast_in_dim.74), channel_id=1, replica_groups=mesh['sp'=16,'tp_0'=4,'tp_1'=2] {'tp_0'}, dimensions={0} | all-to-all | bytes 4194304 | tf_op jit(solution)/shard_map/all_to_all | solution.py:26
  95.9 0.5 broadcast_in_dim.75
  96.4 8.3 %all_to_all.51 = bf16[2,4,128,2048]{3,2,1,0:T(8,128)(2,1)} all-to-all(bf16[2,4,128,2048]{3,2,1,0:T(8,128)(2,1)S(1)} %broadcast_in_dim.75), channel_id=1, replica_groups=mesh['sp'=16,'tp_0'=4,'tp_1'=2] {'tp_1'}, dimensions={0} | all-to-all | bytes 8388608 | tf_op jit(solution)/shard_map/all_to_all | solution.py:26
  104.7 2.2 stack.2
  106.8 4.6 %all-to-all-start.4 = ((bf16[16,704,128]{2,1,0:T(8,128)(2,1)}), bf16[16,704,128]{2,1,0:T(8,128)(2,1)}, u32[]{:S(2)}, u32[]{:S(2)}) async-start(bf16[16,704,128]{2,1,0:T(8,128)(2,1)} %stack.2), calls=%async_computation.4 | async-start | bytes 5767168 | tf_op jit(solution)/shard_map/all_to_all | solution.py:195
  111.5 4.8 %copy.37 = bf16[2,4,128,2048]{3,2,0,1:T(8,128)(2,1)} copy(bf16[2,4,128,2048]{3,2,1,0:T(8,128)(2,1)} %all_to_all.51) | data formatting | bytes 8388608 | tf_op jit(solution)/shard_map/all_to_all | solution.py:26
  116.3 7.8 %fusion.45 = f32[1024,704]{0,1:T(8,128)} fusion(bf16[1024,2048]{1,0:T(8,128)(2,1)} %bitcast.185, bf16[2048,1408]{0,1:T(8,128)(2,1)} %all-gather.2.cloned.1.call-done), kind=kOutput, calls=%fused_computation.58 | convolution fusion | flops 2952790016 | bytes 9961472 | tf_op jit(solution)/shard_map/dot_general | solution.py:229
  124.1 32.4 %all-to-all-done.4 = bf16[16,704,128]{2,1,0:T(8,128)(2,1)} async-done(((bf16[16,704,128]{2,1,0:T(8,128)(2,1)}), bf16[16,704,128]{2,1,0:T(8,128)(2,1)}, u32[]{:S(2)}, u32[]{:S(2)}) %all-to-all-start.4) | async-done | bytes 2883616 | tf_op jit(solution)/shard_map/all_to_all | solution.py:195
  156.6 12.0 %convolution_convert_fusion = bf16[1024,2048]{1,0:T(8,128)(2,1)} fusion(f32[1024,704]{0,1:T(8,128)} %fusion.45, bf16[1024,2048]{1,0:T(8,128)(2,1)} %bitcast.186, bf16[2048,1408]{0,1:T(8,128)(2,1)} %all-gather.2.cloned.1.call-done, bf16[16,704,128]{2,1,0:T(8,128)(2,1)} %all-to-all-done.4), kind=kOutput, calls=%fused_computation.53 | convolution fusion | flops 5912002560 | bytes 17039360 | tf_op jit(solution)/shard_map/dot_general | solution.py:232
  168.6 2.5 %copy.46 = bf16[4,2,128,2048]{3,2,0,1:T(8,128)(2,1)S(1)} copy(bf16[4,2,128,2048]{3,2,1,0:T(8,128)(2,1)} %bitcast.187) | data formatting | bytes 8388608 | tf_op jit(solution)/shard_map/reshape;reshape | solution.py:89
  171.1 8.2 %all_to_all.52 = bf16[2,4,128,2048]{3,2,1,0:T(8,128)(2,1)} all-to-all(bf16[2,4,128,2048]{3,2,1,0:T(8,128)(2,1)S(1)} %bitcast.184), channel_id=1, replica_groups=mesh['sp'=16,'tp_0'=4,'tp_1'=2] {'tp_1'}, dimensions={0} | all-to-all | bytes 8388608 | tf_op jit(solution)/shard_map/all_to_all | solution.py:95
  179.3 3.5 %reduce_sum.41 = bf16[4,128,2048]{2,1,0:T(8,128)(2,1)S(1)} reduce(bf16[2,4,128,2048]{3,2,1,0:T(8,128)(2,1)} %all_to_all.52, bf16[]{:T(256)} %constant.49.clone.1), dimensions={0}, to_apply=%region_5.6 | reduce | flops 1048576 | bytes 6291458 | tf_op jit(solution)/shard_map/reduce_sum | solution.py:96
  182.8 29.4 %all_to_all.53 = bf16[4,128,2048]{2,1,0:T(8,128)(2,1)S(1)} all-to-all(bf16[4,128,2048]{2,1,0:T(8,128)(2,1)S(1)} %reduce_sum.41), channel_id=1, replica_groups=mesh['sp'=16,'tp_0'=4,'tp_1'=2] {'tp_0'}, dimensions={0} | all-to-all | bytes 4194304 | tf_op jit(solution)/shard_map/all_to_all | solution.py:103
  212.2 0.4 convert_reduce_fusion
  212.6 0.9 add_convert_fusion
  (159 shorter events, 8.4 us)
Async XLA Ops:
  6.5 109.8 %all-gather.2.cloned.1.call-start = ((), (), s32[]{:S(2)}) async-start(), calls=%async_computation.7 | async-start | bytes 6127616 | tf_op jit(solution)/shard_map/all_gather | solution.py:17
  29.9 20.2 %all-to-all-start = ((bf16[16,129,128]{2,1,0:T(8,128)(2,1)}), bf16[16,129,128]{2,1,0:T(8,128)(2,1)S(1)}, u32[]{:S(2)}, u32[]{:S(2)}) async-start(bf16[16,129,128]{2,1,0:T(8,128)(2,1)} %broadcast_in_dim.48), calls=%async_computation | async-start | bytes 1114112 | tf_op jit(solution)/shard_map/all_to_all | solution.py:26
  50.2 1.5 copy-start.1
  50.2 1.4 copy-start.4
  50.5 13.1 %copy-start = (bf16[128,2048]{1,0:T(8,128)(2,1)S(1)}, bf16[128,2048]{1,0:T(8,128)(2,1)}, u32[]{:S(2)}) copy-start(bf16[128,2048]{1,0:T(8,128)(2,1)} %param.15) | copy-start | bytes 1572868
  63.6 3.0 %copy-start.3 = (f32[2048]{0:T(1024)S(1)}, f32[2048]{0:T(1024)}, u32[]{:S(2)}) copy-start(f32[2048]{0:T(1024)} %param.24) | copy-start | bytes 24580
  96.4 8.3 %copy-start.2 = (bf16[704,128]{1,0:T(8,128)(2,1)S(1)}, bf16[704,128]{1,0:T(8,128)(2,1)}, u32[]{:S(2)}) copy-start(bf16[704,128]{1,0:T(8,128)(2,1)} %param.27) | copy-start | bytes 540676
  106.8 49.7 %all-to-all-start.4 = ((bf16[16,704,128]{2,1,0:T(8,128)(2,1)}), bf16[16,704,128]{2,1,0:T(8,128)(2,1)}, u32[]{:S(2)}, u32[]{:S(2)}) async-start(bf16[16,704,128]{2,1,0:T(8,128)(2,1)} %stack.2), calls=%async_computation.4 | async-start | bytes 5767168 | tf_op jit(solution)/shard_map/all_to_all | solution.py:195
Sparse Core Ops, SparseCore 0:
  9.4 66.9 all-gather.1
